TPU v7x, 128 devices: a whole 4x4x4 slice. The times are simulated.
128 devices in a mesh: ep: 128 (over z, y, x, core).
Axes of the slice: x: 4, y: 4, z: 4, core: 2. Of those that a mesh axis runs over, the one named last changes fastest.
Arguments:
- tokens: bfloat16 [6144, 2048], P('ep'), may hold values from -6 to 6
- history_length: int32 [6144], P('ep'), may hold values from 1024 to 8192
- norm_gain: float32 [2048], replicated, may hold values from 0.1 to 1.9
- w_query: bfloat16 [2048, 512], replicated, may hold values from -0.125 to 0.125
- w_key: bfloat16 [2048, 512], replicated, may hold values from -0.125 to 0.125
- w_value: bfloat16 [2048, 512], replicated, may hold values from -0.125 to 0.125
- w_gate: bfloat16 [2048, 512], replicated, may hold values from -0.125 to 0.125
- decay_rate: float32 [8], replicated, may hold values from 0.003 to 0.7
- state: float32 [6144, 8, 64, 64], P('ep'), may hold values from -4 to 4
- head_gain: float32 [512], replicated, may hold values from 0.1 to 1.9
- w_out: bfloat16 [512, 2048], replicated, may hold values from -0.25 to 0.25
- moe_gain: float32 [2048], replicated, may hold values from 0.1 to 1.9
- route_weights: float32 [6144, 2], P('ep'), may hold values from 0.3 to 3
- expert_group: int32 [6144], P('ep'), may hold values from 0 to 3, as said below
- expert_inner: int32 [6144, 2], P('ep'), may hold values from 0 to 31, as said below
- expert_gate: bfloat16 [128, 2048, 256], P('ep'), may hold values from -0.125 to 0.125
- expert_up: bfloat16 [128, 2048, 256], P('ep'), may hold values from -0.125 to 0.125
- expert_down: bfloat16 [128, 256, 2048], P('ep'), may hold values from -0.375 to 0.375
Outputs:
- output: bfloat16 [6144, 2048], P('ep')
- new_state: float32 [6144, 8, 64, 64], P('ep')
Inputs may be any that keep to these rules, and one draw needn't show every extreme that they name: `expert_group`: together with expert_inner it names 2 different experts of one group for each token. `expert_inner`: the rows of one device name one expert at most 2 times; in every draw some expert is named exactly 2 times by the rows of every device.
All inputs are finite; a program needn't handle non-finite values.
Results may differ from a plain program's by a relative error of at most 0.02.
Values may be sent and summed in bfloat16 or wider, within the bound.
A program may use at most 128 MiB of HBM per device.

v0:
```python
import jax
import jax.numpy as jnp
from jax import lax
from jax.sharding import PartitionSpec as P

GROUPS = 4
TOP_K = 2


epsilon = 1e-06


def rotate(values, places):
    halfway = values.shape[-1] // 2
    inverse = 10000.0 ** (-jnp.arange(halfway, dtype=jnp.float32) / halfway)
    angles = places[:, None] * inverse[None, :]
    cosine = jnp.cos(angles)[:, None, :]
    sine_table = jnp.sin(angles)[:, None, :]
    first_half = values[..., :halfway]
    second = values[..., halfway:]
    return jnp.concatenate(
        [first_half * cosine - second * sine_table, first_half * sine_table + second * cosine],
        axis=-1,
    )


def rms_scale(values, gains):
    return values * lax.rsqrt(jnp.mean(values * values, axis=-1, keepdims=True) + epsilon) * gains


def retention_step(
    tokens,
    history_length,
    norm_gain,
    w_query,
    w_key,
    w_value,
    w_gate,
    decay_rate,
    state,
    head_gain,
    w_out,
    moe_gain,
):
    row_count = tokens.shape[0]
    head_count = decay_rate.shape[0]
    head_width = state.shape[-1]
    inputs = tokens.astype(jnp.float32)
    normed = rms_scale(inputs, norm_gain).astype(jnp.bfloat16)

    def project(weights):
        return jnp.dot(normed, weights, preferred_element_type=jnp.float32).astype(jnp.bfloat16)

    queries = project(w_query).reshape(row_count, head_count, head_width).astype(jnp.float32)
    keys_now = project(w_key).reshape(row_count, head_count, head_width).astype(jnp.float32)
    values_now = project(w_value).reshape(row_count, head_count, head_width).astype(jnp.float32)
    gating = project(w_gate).astype(jnp.float32)
    places = history_length.astype(jnp.float32)
    queries = rotate(queries, places)
    keys_now = rotate(keys_now, places) * head_width ** (-0.5)
    retain = jnp.exp(-decay_rate)
    new_state = (
        retain[None, :, None, None] * state + keys_now[:, :, :, None] * values_now[:, :, None, :]
    )
    reading = jnp.einsum("bhk,bhkv->bhv", queries, new_state)
    reading = rms_scale(reading, head_gain.reshape(head_count, head_width))
    mixed_heads = (
        reading.reshape(row_count, head_count * head_width) * jax.nn.silu(gating)
    ).astype(jnp.bfloat16)
    mixed_tokens = (
        inputs + jnp.dot(mixed_heads, w_out, preferred_element_type=jnp.float32)
    ).astype(jnp.bfloat16)
    normed_moe = rms_scale(mixed_tokens.astype(jnp.float32), moe_gain).astype(jnp.bfloat16)
    return (mixed_tokens, normed_moe, new_state)


def expert_apply(row_block, gate_weight, up_weight, down_weight):
    gate_part = jnp.dot(row_block, gate_weight, preferred_element_type=jnp.float32)
    up_part = jnp.dot(row_block, up_weight, preferred_element_type=jnp.float32)
    hidden = (jax.nn.silu(gate_part) * up_part).astype(jnp.bfloat16)
    return jnp.dot(hidden, down_weight, preferred_element_type=jnp.float32).astype(jnp.bfloat16)


def slot_positions(flat_ids, experts):
    onehot = (flat_ids[:, None] == jnp.arange(experts, dtype=jnp.int32)[None, :]).astype(jnp.int32)
    earlier = jnp.cumsum(onehot, axis=0) - onehot
    return jnp.sum(earlier * onehot, axis=1)


def local(
    tokens,
    history_length,
    norm_gain,
    w_query,
    w_key,
    w_value,
    w_gate,
    decay_rate,
    state,
    head_gain,
    w_out,
    moe_gain,
    route_weights,
    expert_group,
    expert_inner,
    expert_gate,
    expert_up,
    expert_down,
):
    experts = lax.axis_size("ep")
    per_group = experts // GROUPS
    seq_count = tokens.shape[0]
    capacity = max(2, 4 * seq_count // experts)
    model_width = tokens.shape[1]
    expert_ids = expert_group[:, None] * per_group + expert_inner
    mixed_tokens, normed_moe, new_state = retention_step(
        tokens,
        history_length,
        norm_gain,
        w_query,
        w_key,
        w_value,
        w_gate,
        decay_rate,
        state,
        head_gain,
        w_out,
        moe_gain,
    )
    flat_ids = expert_ids.reshape(-1)
    target = flat_ids * capacity + slot_positions(flat_ids, experts)
    placement_table = (
        target[:, None] == jnp.arange(experts * capacity, dtype=jnp.int32)[None, :]
    ).astype(jnp.bfloat16)
    repeated = jnp.repeat(normed_moe, TOP_K, axis=0)
    outgoing = jnp.einsum(
        "rs,rd->sd", placement_table, repeated, preferred_element_type=jnp.float32
    )
    outgoing = outgoing.astype(jnp.bfloat16).reshape(experts, capacity, model_width)
    incoming = lax.all_to_all(outgoing, "ep", split_axis=0, concat_axis=0, tiled=True)
    flat_rows = incoming.reshape(-1, model_width)
    outputs = expert_apply(flat_rows, expert_gate[0], expert_up[0], expert_down[0]).reshape(
        incoming.shape
    )
    returned_rows = lax.all_to_all(outputs, "ep", split_axis=0, concat_axis=0, tiled=True)
    collected = jnp.einsum(
        "rs,sd->rd",
        placement_table,
        returned_rows.reshape(experts * capacity, model_width),
        preferred_element_type=jnp.float32,
    )
    collected = collected.reshape(-1, TOP_K, model_width)
    routed = jnp.sum(collected * route_weights[:, :, None], axis=1)
    output = (mixed_tokens.astype(jnp.float32) + routed).astype(jnp.bfloat16)
    return (output, new_state)


def solution(mesh):
    return jax.shard_map(
        local,
        mesh=mesh,
        in_specs=(
            P("ep", None),
            P("ep"),
            P(),
            P(),
            P(),
            P(),
            P(),
            P(),
            P("ep", None, None, None),
            P(),
            P(),
            P(),
            P("ep", None),
            P("ep"),
            P("ep", None),
            P("ep", None, None),
            P("ep", None, None),
            P("ep", None, None),
        ),
        out_specs=(P("ep", None), P("ep", None, None, None)),
        check_vma=False,
    )
```

profile of v0, /device:TPU:1, one launch (start us, length us, event | category | flops | bytes accessed | tf_op | source)
XLA Modules:
  0.0 104.1 jit_solution(1224752899276910808)
XLA Ops:
  0.7 0.8 broadcast_multiply_fusion
  1.5 0.7 convert_element_type.80
  2.2 0.7 negate_exponential_fusion
  2.8 1.1 %fusion.13 = f32[48]{0:T(128)S(1)} fusion(bf16[48,2048]{1,0:T(8,128)(2,1)} %param.18), kind=kLoop, calls=%fused_computation.24 | loop fusion | flops 294864 | bytes 196800 | tf_op jit(solution)/shard_map/reduce_sum | solution.py:28
  3.9 0.8 mul.244
  4.7 0.7 broadcast_add_fusion
  5.8 0.2 select_reduce_fusion
  6.0 2.2 %fusion.6 = f32[48,512]{1,0:T(8,128)S(1)} fusion(bf16[2048,512]{1,0:T(8,128)(2,1)} %param.22, bf16[48,2048]{1,0:T(8,128)(2,1)} %param.18, f32[2048]{0:T(1024)} %param.20, f32[48]{0:T(128)S(1)} %add_rsqrt_fusion.2), kind=kOutput, calls=%fused_computation.15 | convolution fusion | flops 101105664 | bytes 2400448 | tf_op jit(solution)/shard_map/dot_general | solution.py:52
  8.3 2.1 %fusion.5 = f32[48,512]{1,0:T(8,128)S(1)} fusion(bf16[2048,512]{1,0:T(8,128)(2,1)} %param.23, bf16[48,2048]{1,0:T(8,128)(2,1)S(1)} %copy-done.2, f32[2048]{0:T(1024)S(1)} %copy-done.4, f32[48]{0:T(128)S(1)} %add_rsqrt_fusion.2), kind=kOutput, calls=%fused_computation.13 | convolution fusion | flops 101105664 | bytes 2400448 | tf_op jit(solution)/shard_map/dot_general | solution.py:52
  10.5 2.1 %fusion.7 = f32[48,512]{1,0:T(8,128)S(1)} fusion(bf16[2048,512]{1,0:T(8,128)(2,1)} %param.21, bf16[48,2048]{1,0:T(8,128)(2,1)S(1)} %copy-done.2, f32[2048]{0:T(1024)S(1)} %copy-done.4, f32[48]{0:T(128)S(1)} %add_rsqrt_fusion.2), kind=kOutput, calls=%fused_computation.17 | convolution fusion | flops 101105664 | bytes 2400448 | tf_op jit(solution)/shard_map/dot_general | solution.py:52
  12.8 0.2 multiply_cosine_fusion
  12.9 0.2 multiply_subtract_fusion
  13.2 0.2 pad_maximum_fusion
  13.3 8.5 %multiply_add_fusion = f32[48,8,64,64]{3,2,1,0:T(8,128)S(1)} fusion(f32[48,8,64,64]{3,2,1,0:T(8,128)} %param.26, f32[48,8,64]{2,1,0:T(8,128)S(1)} %reshape.176, f32[48,8,64]{2,1,0:T(8,128)S(1)} %get-tuple-element.13, f32[8]{0:T(128)S(1)} %negate_exponential_fusion), kind=kLoop, calls=%fused_computation | loop fusion | flops 4718592 | bytes 12779552 | tf_op jit(solution)/shard_map/add | solution.py:63
  21.8 1.8 %fusion.37 = f32[48,8,1,64]{3,2,1,0:T(1,128)S(1)} fusion(f32[48,8,64,1]{2,3,1,0:T(1,128)S(1)} %bitcast.31, f32[48,8,64,64]{3,2,1,0:T(8,128)S(1)} %multiply_add_fusion), kind=kOutput, calls=%fused_computation.67 | convolution fusion | flops 3145728 | bytes 6488064 | tf_op jit(solution)/shard_map/bhk,bhkv->bhv/dot_general | solution.py:65
  23.6 3.0 %copy-done.1 = f32[48,8,64,64]{3,2,1,0:T(8,128)} copy-done((f32[48,8,64,64]{3,2,1,0:T(8,128)}, f32[48,8,64,64]{3,2,1,0:T(8,128)S(1)}, u32[]{:S(2)}) %copy-start.1) | copy-done | bytes 6291480
  27.1 2.7 %multiply_reduce_fusion = (f32[48]{0:T(128)S(1)}, f32[48,2048]{1,0:T(8,128)S(1)}) fusion(bf16[512,2048]{1,0:T(8,128)(2,1)S(1)} %copy-done, f32[48,512]{1,0:T(8,128)S(1)} %reshape.168, bf16[2048,512]{1,0:T(8,128)(2,1)} %param.24, bf16[48,2048]{1,0:T(8,128)(2,1)S(1)} %copy-done.2, f32[2048]{0:T(1024)S(1)} %copy-done.4, f32[48]{0:T(128)S(1)} %add_rsqrt_fusion.2), kind=kOutput, calls=%fused_computation.29 | convolution fusion | flops 202506192 | bytes 4891008 | tf_op jit(solution)/shard_map/dot_general | solution.py:71
  30.0 0.2 broadcast_in_dim.2
  30.2 0.4 copy-done.3
  30.6 0.9 reshape.169
  31.5 1.5 %convolution_convert_fusion = bf16[256,2048]{1,0:T(8,128)(2,1)S(1)} fusion(bf16[96,2048]{1,0:T(8,128)(2,1)} %reshape.169, s32[96]{0:T(128)S(1)} %multiply_add_fusion.4), kind=kOutput, calls=%fused_computation.1 | convolution fusion | flops 101212160 | bytes 1442176 | tf_op jit(solution)/shard_map/rs,rd->sd/dot_general | solution.py:136
  33.0 1.5 %reshape.170 = bf16[128,2,2048]{2,1,0:T(2,128)(2,1)} reshape(bf16[256,2048]{1,0:T(8,128)(2,1)S(1)} %convolution_convert_fusion) | data formatting | bytes 2097152 | tf_op jit(solution)/shard_map/reshape | solution.py:139
  34.5 30.8 %all_to_all.10 = bf16[128,2,2048]{2,1,0:T(2,128)(2,1)} all-to-all(bf16[128,2,2048]{2,1,0:T(2,128)(2,1)} %reshape.170), channel_id=1, replica_groups=mesh['ep'=128] {'ep'}, dimensions={0} | all-to-all | bytes 2097152 | tf_op jit(solution)/shard_map/all_to_all | solution.py:140
  65.4 1.5 %reshape.171 = bf16[256,2048]{1,0:T(8,128)(2,1)S(1)} reshape(bf16[128,2,2048]{2,1,0:T(2,128)(2,1)} %all_to_all.10) | data formatting | bytes 2097152 | tf_op jit(solution)/shard_map/reshape | solution.py:141
  66.8 2.4 %fusion.11 = f32[256,256]{1,0:T(8,128)} fusion(bf16[256,2048]{1,0:T(8,128)(2,1)S(1)} %reshape.171, bf16[1,2048,256]{2,1,0:T(8,128)(2,1)} %param.33), kind=kOutput, calls=%fused_computation.20 | convolution fusion | flops 268435456 | bytes 2359296 | tf_op jit(solution)/shard_map/dot_general | solution.py:78
  69.2 3.9 %convolution_convert_fusion.1 = bf16[256,2048]{1,0:T(8,128)(2,1)} fusion(bf16[256,2048]{1,0:T(8,128)(2,1)S(1)} %reshape.171, bf16[1,256,2048]{2,1,0:T(8,128)(2,1)} %param.35, bf16[1,2048,256]{2,1,0:T(8,128)(2,1)} %param.34, f32[256,256]{1,0:T(8,128)} %fusion.11), kind=kOutput, calls=%fused_computation.2 | convolution fusion | flops 537788416 | bytes 4456448 | tf_op jit(solution)/shard_map/dot_general | solution.py:81
  73.1 2.6 %reshape.172 = bf16[128,2,2048]{2,1,0:T(2,128)(2,1)} reshape(bf16[256,2048]{1,0:T(8,128)(2,1)} %convolution_convert_fusion.1) | data formatting | bytes 2097152 | tf_op jit(solution)/shard_map/reshape | solution.py:142
  75.7 4.5 %all-to-all-start.1 = ((bf16[128,2,2048]{2,1,0:T(2,128)(2,1)}), bf16[128,2,2048]{2,1,0:T(2,128)(2,1)S(1)}, u32[]{:S(2)}, u32[]{:S(2)}) async-start(bf16[128,2,2048]{2,1,0:T(2,128)(2,1)} %reshape.172), calls=%async_computation.1 | async-start | bytes 2097152 | tf_op jit(solution)/shard_map/all_to_all | solution.py:145
  80.4 19.2 %all-to-all-done.1 = bf16[128,2,2048]{2,1,0:T(2,128)(2,1)S(1)} async-done(((bf16[128,2,2048]{2,1,0:T(2,128)(2,1)}), bf16[128,2,2048]{2,1,0:T(2,128)(2,1)S(1)}, u32[]{:S(2)}, u32[]{:S(2)}) %all-to-all-start.1) | async-done | bytes 1048608 | tf_op jit(solution)/shard_map/all_to_all | solution.py:145
  99.6 1.2 %reshape.179 = bf16[256,2048,1]{1,0,2:T(8,128)(2,1)} reshape(bf16[128,2,2048]{2,1,0:T(2,128)(2,1)S(1)} %all-to-all-done.1) | data formatting | bytes 2097152 | tf_op jit(solution)/shard_map/reshape | solution.py:149
  100.8 1.6 %fusion.2 = f32[48,2048]{1,0:T(8,128)S(1)} fusion(bf16[256,2048,1]{1,0,2:T(8,128)(2,1)} %reshape.179, f32[48,2]{0,1:T(2,128)S(1)} %copy-done.7, s32[48,2]{0,1:T(2,128)S(1)} %multiply_add_fusion.3), kind=kOutput, calls=%fused_computation.7 | convolution fusion | flops 100982784 | bytes 1442560 | tf_op jit(solution)/shard_map/rs,sd->rd/dot_general | solution.py:146
  102.4 1.7 %add_convert_fusion = bf16[48,2048]{1,0:T(8,128)(2,1)} fusion(f32[48,2048]{1,0:T(8,128)} %copy-done.3, f32[48,2048]{1,0:T(8,128)S(1)} %fusion.2), kind=kLoop, calls=%fused_computation.27 | loop fusion | flops 196608 | bytes 983040 | tf_op jit(solution)/shard_map/convert_element_type | solution.py:154
  (35 shorter events, 1.6 us)
Async XLA Ops:
  0.6 26.5 %copy-start = (bf16[512,2048]{1,0:T(8,128)(2,1)S(1)}, bf16[512,2048]{1,0:T(8,128)(2,1)}, u32[]{:S(2)}) copy-start(bf16[512,2048]{1,0:T(8,128)(2,1)} %param.28) | copy-start | bytes 6291460
  0.6 7.7 %copy-start.2 = (bf16[48,2048]{1,0:T(8,128)(2,1)S(1)}, bf16[48,2048]{1,0:T(8,128)(2,1)}, u32[]{:S(2)}) copy-start(bf16[48,2048]{1,0:T(8,128)(2,1)} %param.18) | copy-start | bytes 589828
  0.7 7.7 %copy-start.4 = (f32[2048]{0:T(1024)S(1)}, f32[2048]{0:T(1024)}, u32[]{:S(2)}) copy-start(f32[2048]{0:T(1024)} %param.20) | copy-start | bytes 24580
  21.8 4.8 %copy-start.1 = (f32[48,8,64,64]{3,2,1,0:T(8,128)}, f32[48,8,64,64]{3,2,1,0:T(8,128)S(1)}, u32[]{:S(2)}) copy-start(f32[48,8,64,64]{3,2,1,0:T(8,128)S(1)} %multiply_add_fusion) | copy-start | bytes 18874372
  27.1 2.7 %copy-start.5 = (f32[2048]{0:T(1024)S(1)}, f32[2048]{0:T(1024)}, u32[]{:S(2)}) copy-start(f32[2048]{0:T(1024)} %param.29) | copy-start | bytes 24580
  29.8 0.8 copy-start.3
  73.1 7.3 %copy-start.6 = (s32[48,2]{0,1:T(2,128)S(1)}, s32[48,2]{0,1:T(2,128)}, u32[]{:S(2)}) copy-start(s32[48,2]{0,1:T(2,128)} %param.32) | copy-start | bytes 1156
  75.7 25.1 %copy-start.7 = (f32[48,2]{0,1:T(2,128)S(1)}, f32[48,2]{0,1:T(2,128)}, u32[]{:S(2)}) copy-start(f32[48,2]{0,1:T(2,128)} %param.30) | copy-start | bytes 1156
  75.7 23.9 %all-to-all-start.1 = ((bf16[128,2,2048]{2,1,0:T(2,128)(2,1)}), bf16[128,2,2048]{2,1,0:T(2,128)(2,1)S(1)}, u32[]{:S(2)}, u32[]{:S(2)}) async-start(bf16[128,2,2048]{2,1,0:T(2,128)(2,1)} %reshape.172), calls=%async_computation.1 | async-start | bytes 2097152 | tf_op jit(solution)/shard_map/all_to_all | solution.py:145
where the time goes:
time: 105 us; the launch traced here: 104 us
  blocking collectives  30.8 us (29%)
  matrix products  20.3 us (19%)
  waiting for transfers between devices  19.2 us (18%)
  other arithmetic  15.4 us (15%)
  local copies, waits for them, and re-layouts  13 us (12%)
  starting transfers between devices  4.52 us (4%)
    all_to_all x1, blocking collectives, local(): lax.all_to_all(outgoing, 'ep', split_axis=0, concat_axis=0, tiled=True)  30.8 us
    all_to_all x1, waiting for transfers between devices, local(): lax.all_to_all(outputs, 'ep', split_axis=0, concat_axis=0, tiled=True)  19.2 us
    add x1, other arithmetic, retention_step(): retain[None, :, None, None] * state  8.48 us
    dot_general x3, matrix products, project(): jnp.dot(normed, weights, preferred_element_type=jnp.float32)  6.44 us
    all_to_all x1, starting transfers between devices, local(): lax.all_to_all(outputs, 'ep', split_axis=0, concat_axis=0, tiled=True)  4.52 us
    dot_general x1, matrix products, expert_apply(): jnp.dot(hidden, down_weight, preferred_element_type=jnp.float32)  3.91 us
    unnamed x16, local copies, waits for them, and re-layouts  3.43 us
    dot_general x1, matrix products, retention_step(): jnp.dot(mixed_heads, w_out, preferred_element_type=jnp.float32)  2.67 us
  transfers between devices with their start and end apart: 1, of which 1 were waited for; matrix products, arithmetic and copies ran while one was open for 0% of the time, Pallas kernels for 0%

commit v1 on v0

v1 whole, which is shorter than its diff:
```python
import functools

import jax
import jax.numpy as jnp
from jax import lax
from jax.experimental import pallas as pl
from jax.experimental.pallas import tpu as pltpu
from jax.sharding import PartitionSpec as P

MESH = pl.DeviceIdType.MESH
F32 = jnp.float32
BF16 = jnp.bfloat16
GROUP_SIZE = 32
CHUNKS = 4
epsilon = 1e-06


def rotate(values, places):
    halfway = values.shape[-1] // 2
    inverse = 10000.0 ** (-jnp.arange(halfway, dtype=jnp.float32) / halfway)
    angles = places[:, None] * inverse[None, :]
    cosine = jnp.cos(angles)[:, None, :]
    sine_table = jnp.sin(angles)[:, None, :]
    first_half = values[..., :halfway]
    second = values[..., halfway:]
    return jnp.concatenate(
        [first_half * cosine - second * sine_table, first_half * sine_table + second * cosine],
        axis=-1,
    )


def rms_scale(values, gains):
    return values * lax.rsqrt(jnp.mean(values * values, axis=-1, keepdims=True) + epsilon) * gains


def retention_step(
    tokens, history_length, norm_gain, w_query, w_key, w_value, w_gate, decay_rate, state,
    head_gain, w_out, moe_gain,
):
    row_count = tokens.shape[0]
    head_count = decay_rate.shape[0]
    head_width = state.shape[-1]
    inputs = tokens.astype(jnp.float32)
    normed = rms_scale(inputs, norm_gain).astype(jnp.bfloat16)

    def project(weights):
        return jnp.dot(normed, weights, preferred_element_type=jnp.float32).astype(jnp.bfloat16)

    queries = project(w_query).reshape(row_count, head_count, head_width).astype(jnp.float32)
    keys_now = project(w_key).reshape(row_count, head_count, head_width).astype(jnp.float32)
    values_now = project(w_value).reshape(row_count, head_count, head_width).astype(jnp.float32)
    gating = project(w_gate).astype(jnp.float32)
    places = history_length.astype(jnp.float32)
    queries = rotate(queries, places)
    keys_now = rotate(keys_now, places) * head_width ** (-0.5)
    retain = jnp.exp(-decay_rate)
    new_state = (
        retain[None, :, None, None] * state + keys_now[:, :, :, None] * values_now[:, :, None, :]
    )
    reading = jnp.einsum("bhk,bhkv->bhv", queries, new_state)
    reading = rms_scale(reading, head_gain.reshape(head_count, head_width))
    mixed_heads = (
        reading.reshape(row_count, head_count * head_width) * jax.nn.silu(gating)
    ).astype(jnp.bfloat16)
    mixed_tokens = (
        inputs + jnp.dot(mixed_heads, w_out, preferred_element_type=jnp.float32)
    ).astype(jnp.bfloat16)
    normed_moe = rms_scale(mixed_tokens.astype(jnp.float32), moe_gain).astype(jnp.bfloat16)
    return (mixed_tokens, normed_moe, new_state)


def far_first(t):
    return (2 + 3 * ((t * (t + 1)) // 2)) % 4


def digits(me):
    return me // 32, (me // 8) % 4, (me // 2) % 4, me % 2


def partner(me, j, sign):
    z, y, x, c = digits(me)
    dz, dy, dx = far_first(j // 32), far_first((j // 8) % 4), far_first((j // 2) % 4)
    return (
        ((z + 4 + sign * dz) % 4) * 32
        + ((y + 4 + sign * dy) % 4) * 8
        + ((x + 4 + sign * dx) % 4) * 2
        + (c + 1 - j % 2) % 2
    )


def slot_experts(me, r):
    z, y, x, c = digits(me)
    j = r >> 1

    def far(t):
        return (2 + 3 * ((t * (t + 1)) >> 1)) & 3

    return (
        ((z + far(j >> 5)) & 3) * 32
        + ((y + far((j >> 3) & 3)) & 3) * 8
        + ((x + far((j >> 1) & 3)) & 3) * 2
        + ((c + 1 - (j & 1)) & 1)
    )


def moe_kernel(
    normed_ref, mixed_ref, group_ref, inner_ref, route_ref, gate_hbm, up_hbm, down_hbm, out_ref,
    gate_w, up_w, down_w, outgoing, incoming, results, returned,
    weight_sems, send_one, recv_one, send_two, recv_two,
):
    me = lax.axis_index("ep")
    rows = normed_ref.shape[0]
    n = outgoing.shape[0]
    slots = 2 * n
    per = n // CHUNKS
    loads = [
        pltpu.make_async_copy(src.at[0], dst, weight_sems.at[i])
        for i, (src, dst) in enumerate(((gate_hbm, gate_w), (up_hbm, up_w), (down_hbm, down_w)))
    ]
    for load in loads:
        load.start()
    barrier = pltpu.get_barrier_semaphore()

    def greet(j, carry):
        pl.semaphore_signal(barrier, inc=1, device_id=(partner(me, j, 1),), device_id_type=MESH)
        return carry

    lax.fori_loop(0, n - 1, greet, 0)

    first_row = group_ref[...] * GROUP_SIZE + inner_ref[0:1, :]
    second_row = group_ref[...] * GROUP_SIZE + inner_ref[1:2, :]
    sub = lax.broadcasted_iota(jnp.int32, (rows, rows), 0)
    lane = lax.broadcasted_iota(jnp.int32, (rows, rows), 1)

    def column(row):
        return jnp.sum(jnp.where(sub == lane, row, jnp.zeros_like(row)), axis=1, keepdims=True)

    first_col, second_col = column(first_row), column(second_row)

    def rank(ids_row):
        same = (first_col == ids_row).astype(F32) + (second_col == ids_row).astype(F32)
        return jnp.sum(jnp.where(sub < lane, same, 0.0), axis=0, keepdims=True)

    first_rank, second_rank = rank(first_row), rank(second_row)
    r_col = lax.broadcasted_iota(jnp.int32, (slots, 1), 0)
    expert_col = slot_experts(me, r_col)
    k_col = (r_col & 1).astype(F32)
    place = ((expert_col == first_row) & (k_col == first_rank)) | (
        (expert_col == second_row) & (k_col == second_rank)
    )
    place = place.astype(F32).astype(BF16)
    outgoing[...] = (
        jnp.dot(place, normed_ref[...], preferred_element_type=F32)
        .astype(BF16)
        .reshape(n, 2, normed_ref.shape[1])
    )
    pl.semaphore_wait(barrier, n - 1)

    def dispatch(j, carry):
        pltpu.make_async_remote_copy(
            src_ref=outgoing.at[j], dst_ref=incoming.at[j], send_sem=send_one,
            recv_sem=recv_one.at[j // per], device_id=(partner(me, j, 1),), device_id_type=MESH,
        ).start()
        return carry

    lax.fori_loop(0, n - 1, dispatch, 0)
    incoming[n - 1] = outgoing[n - 1]
    for load in loads:
        load.wait()

    def give_back(j, carry):
        pltpu.make_async_remote_copy(
            src_ref=results.at[j], dst_ref=returned.at[j], send_sem=send_two,
            recv_sem=recv_two.at[j // per], device_id=(partner(me, j, -1),), device_id_type=MESH,
        ).start()
        return carry

    def wait_block(ref, sem, start, count):
        block = ref.at[pl.ds(start, count)]
        pltpu.make_async_copy(block, block, sem).wait()

    for chunk in range(CHUNKS):
        start = chunk * per
        count = per if chunk < CHUNKS - 1 else per - 1
        wait_block(incoming, recv_one.at[chunk], start, count)
        x = incoming[pl.ds(start, per)].reshape(2 * per, incoming.shape[2])
        gate_part = jnp.dot(x, gate_w[...], preferred_element_type=F32)
        up_part = jnp.dot(x, up_w[...], preferred_element_type=F32)
        hidden = (gate_part * jax.nn.sigmoid(gate_part) * up_part).astype(BF16)
        y = jnp.dot(hidden, down_w[...], preferred_element_type=F32).astype(BF16)
        results[pl.ds(start, per)] = y.reshape(per, 2, y.shape[1])
        lax.fori_loop(start, start + count, give_back, 0)
    returned[n - 1] = results[n - 1]

    r_row = lax.broadcasted_iota(jnp.int32, (1, slots), 1)
    expert_row = slot_experts(me, r_row)
    k_row = (r_row & 1).astype(F32)
    route_one, route_two = column(route_ref[0:1, :]), column(route_ref[1:2, :])
    first_k, second_k = column(first_rank), column(second_rank)
    weights = jnp.where(
        (first_col == expert_row) & (first_k == k_row), route_one, 0.0
    ) + jnp.where((second_col == expert_row) & (second_k == k_row), route_two, 0.0)
    high = weights.astype(BF16)
    low = (weights - high.astype(F32)).astype(BF16)
    for chunk in range(CHUNKS):
        start = chunk * per
        count = per if chunk < CHUNKS - 1 else per - 1
        wait_block(returned, recv_two.at[chunk], start, count)
    back = returned[...].reshape(slots, returned.shape[2])
    routed = jnp.dot(high, back, preferred_element_type=F32) + jnp.dot(
        low, back, preferred_element_type=F32
    )
    out_ref[...] = (mixed_ref[...].astype(F32) + routed).astype(BF16)
    wait_block(outgoing, send_one, 0, n - 1)
    wait_block(results, send_two, 0, n - 1)


def local(
    tokens, history_length, norm_gain, w_query, w_key, w_value, w_gate, decay_rate, state,
    head_gain, w_out, moe_gain, route_weights, expert_group, expert_inner, expert_gate,
    expert_up, expert_down,
):
    experts = lax.axis_size("ep")
    rows, width = tokens.shape
    hidden = expert_gate.shape[2]
    mixed_tokens, normed_moe, new_state = retention_step(
        tokens, history_length, norm_gain, w_query, w_key, w_value, w_gate, decay_rate, state,
        head_gain, w_out, moe_gain,
    )
    vmem = pl.BlockSpec(memory_space=pltpu.VMEM)
    hbm = pl.BlockSpec(memory_space=pl.ANY)
    slab = pltpu.VMEM((experts, 2, width), BF16)
    output = pl.pallas_call(
        moe_kernel,
        out_shape=jax.ShapeDtypeStruct((rows, width), BF16),
        in_specs=[vmem] * 5 + [hbm] * 3,
        out_specs=vmem,
        scratch_shapes=[
            pltpu.VMEM((width, hidden), BF16),
            pltpu.VMEM((width, hidden), BF16),
            pltpu.VMEM((hidden, width), BF16),
            slab, slab, slab, slab,
            pltpu.SemaphoreType.DMA((3,)),
            pltpu.SemaphoreType.DMA,
            pltpu.SemaphoreType.DMA((CHUNKS,)),
            pltpu.SemaphoreType.DMA,
            pltpu.SemaphoreType.DMA((CHUNKS,)),
        ],
        compiler_params=pltpu.CompilerParams(
            collective_id=0, has_side_effects=True, vmem_limit_bytes=40 * 1024 * 1024
        ),
    )(
        normed_moe, mixed_tokens, expert_group.reshape(1, rows), expert_inner.T,
        route_weights.T, expert_gate, expert_up, expert_down,
    )
    return (output, new_state)


def solution(mesh):
    return jax.shard_map(
        local,
        mesh=mesh,
        in_specs=(
            P("ep", None), P("ep"), P(), P(), P(), P(), P(), P(), P("ep", None, None, None),
            P(), P(), P(), P("ep", None), P("ep"), P("ep", None), P("ep", None, None),
            P("ep", None, None), P("ep", None, None),
        ),
        out_specs=(P("ep", None), P("ep", None, None, None)),
        check_vma=False,
    )
```

time: 105 us -> 80.7 us (0.77)
  Pallas kernels: 0 us -> 48.9 us
  blocking collectives: 30.8 us -> 0 us
  waiting for transfers between devices: 19.2 us -> 0 us
  matrix products: 20.3 us -> 9.95 us
  starting transfers between devices: 4.52 us -> 0 us
  local copies, waits for them, and re-layouts: 13 us -> 8.57 us
  other arithmetic: 15.4 us -> 12 us
    pallas_call x0 -> x1, Pallas kernels: none -> 48.9 us  [local(): pl.pallas_call(moe_kernel, out_shape=jax.ShapeDtypeStruct((rows, width),...]
    all_to_all x1 -> x0, blocking collectives: 30.8 us -> none  [local(): lax.all_to_all(outgoing, 'ep', split_axis=0, concat_axis=0, tiled=True)]
    all_to_all x1 -> x0, waiting for transfers between devices: 19.2 us -> none  [local(): lax.all_to_all(outputs, 'ep', split_axis=0, concat_axis=0, tiled=True)]
    dot_general x4 -> x0, matrix products: 9.42 us -> none  [the longest x1 3.91 us: expert_apply(): jnp.dot(hidden, down_weight, preferred_element_type=jnp.float32)]
    reshape x5 -> x0, local copies, waits for them, and re-layouts: 7.64 us -> none  [the longest x1 2.56 us: local(): expert_apply(flat_rows, expert_gate[0], expert_up[0], expert_down[0])]
    all_to_all x1 -> x0, starting transfers between devices: 4.52 us -> none  [local(): lax.all_to_all(outputs, 'ep', split_axis=0, concat_axis=0, tiled=True)]
    unnamed x16 -> x29, local copies, waits for them, and re-layouts: 3.43 us -> 7.32 us
    convert_element_type x2 -> x0, other arithmetic: 1.81 us -> none  [the longest x1 1.73 us: local(): output = (mixed_tokens.astype(jnp.float32) + routed).astype(jnp.bfloat16)]
  transfers between devices with their start and end apart: 1 -> 0, of which waited for: 1 -> 0; matrix products, arithmetic and copies ran while one was open for 0% -> 0% of each run, Pallas kernels for 0% -> 0%
where the time goes in v1:
time: 80.7 us; the launch traced here: 80.3 us
  Pallas kernels  48.9 us (61%)
  other arithmetic  12 us (15%)
  matrix products  9.95 us (12%)
  local copies, waits for them, and re-layouts  8.57 us (11%)
  between operations  0.88 us (1%)
    pallas_call x1, Pallas kernels, local(): pl.pallas_call(moe_kernel, out_shape=jax.ShapeDtypeStruct((rows, width),...  48.9 us
    add x1, other arithmetic, retention_step(): retain[None, :, None, None] * state  8.47 us
    unnamed x29, local copies, waits for them, and re-layouts  7.32 us
    dot_general x3, matrix products, project(): jnp.dot(normed, weights, preferred_element_type=jnp.float32)  4.85 us
    dot_general x1, matrix products, retention_step(): jnp.dot(mixed_heads, w_out, preferred_element_type=jnp.float32)  3.33 us
    dot_general x1, matrix products, retention_step(): reading = jnp.einsum('bhk,bhkv->bhv', queries, new_state)  1.78 us

profile of v1, /device:TPU:1, one launch (start us, length us, event | category | flops | bytes accessed | tf_op | source)
XLA Modules:
  0.0 80.3 jit_solution(12894452753436610014)
XLA Ops:
  0.6 0.0 copy-start
  0.6 0.0 copy-start.8
  0.7 0.0 copy-start.10
  0.7 1.2 %fusion.8 = f32[48]{0:T(128)S(1)} fusion(bf16[48,2048]{1,0:T(8,128)(2,1)} %param.18), kind=kLoop, calls=%fused_computation.18 | loop fusion | flops 294864 | bytes 196800 | tf_op jit(solution)/shard_map/reduce_sum | solution.py:33
  1.9 2.2 %fusion.3 = f32[48,512]{1,0:T(8,128)S(1)} fusion(bf16[2048,512]{1,0:T(8,128)(2,1)} %param.22, bf16[48,2048]{1,0:T(8,128)(2,1)} %param.18, f32[2048]{0:T(1024)} %param.20, f32[48]{0:T(128)S(1)} %add_rsqrt_fusion.2), kind=kOutput, calls=%fused_computation.8 | convolution fusion | flops 101105664 | bytes 2400448 | tf_op jit(solution)/shard_map/dot_general | solution.py:47
  4.2 0.1 reshape.121
  4.3 0.2 multiply_cosine_fusion
  4.5 2.1 %fusion.4 = f32[48,512]{1,0:T(8,128)S(1)} fusion(bf16[2048,512]{1,0:T(8,128)(2,1)} %param.21, bf16[48,2048]{1,0:T(8,128)(2,1)S(1)} %copy-done.8, f32[2048]{0:T(1024)S(1)} %copy-done.10, f32[48]{0:T(128)S(1)} %add_rsqrt_fusion.2), kind=kOutput, calls=%fused_computation.10 | convolution fusion | flops 101105664 | bytes 2400448 | tf_op jit(solution)/shard_map/dot_general | solution.py:47
  6.6 0.1 reshape.120
  6.7 0.2 multiply_subtract_fusion
  7.0 0.2 pad_maximum_fusion
  7.1 1.2 %copy-done.9 = bf16[2048,512]{1,0:T(8,128)(2,1)S(1)} copy-done((bf16[2048,512]{1,0:T(8,128)(2,1)S(1)}, bf16[2048,512]{1,0:T(8,128)(2,1)}, u32[]{:S(2)}) %copy-start.9) | copy-done | bytes 2097176
  8.3 0.5 fusion.2
  8.8 0.1 reshape.122
  8.9 8.5 %multiply_add_fusion = f32[48,8,64,64]{3,2,1,0:T(8,128)S(1)} fusion(f32[48,8,64,64]{3,2,1,0:T(8,128)} %param.26, f32[48,8,64]{2,1,0:T(8,128)S(1)} %reshape.122, f32[48,8,64]{2,1,0:T(8,128)S(1)} %get-tuple-element.13, f32[8]{0:T(128)S(1)} %negate_exponential_fusion), kind=kLoop, calls=%fused_computation | loop fusion | flops 4718592 | bytes 12779552 | tf_op jit(solution)/shard_map/add | solution.py:58
  17.4 0.0 copy-start.7
  17.4 0.0 copy-start.11
  17.4 1.8 %fusion.20 = f32[48,8,1,64]{3,2,1,0:T(1,128)S(1)} fusion(f32[48,8,64,1]{2,3,1,0:T(1,128)S(1)} %bitcast.20, f32[48,8,64,64]{3,2,1,0:T(8,128)S(1)} %multiply_add_fusion), kind=kOutput, calls=%fused_computation.39 | convolution fusion | flops 3145728 | bytes 6488064 | tf_op jit(solution)/shard_map/bhk,bhkv->bhv/dot_general | solution.py:60
  19.2 3.0 %copy-done.7 = f32[48,8,64,64]{3,2,1,0:T(8,128)} copy-done((f32[48,8,64,64]{3,2,1,0:T(8,128)}, f32[48,8,64,64]{3,2,1,0:T(8,128)S(1)}, u32[]{:S(2)}) %copy-start.7) | copy-done | bytes 6291480
  22.2 0.1 mul.204
  22.3 0.1 multiply_reduce_fusion
  22.4 0.1 copy.21
  22.5 0.1 copy.22
  22.5 0.1 multiply_multiply_fusion
  22.7 0.7 reshape.118
  23.4 3.3 %fusion.5 = (f32[48]{0:T(128)}, bf16[48,2048]{1,0:T(8,128)(2,1)S(1)}) fusion(bf16[512,2048]{1,0:T(8,128)(2,1)S(1)} %copy-done, f32[48,512]{1,0:T(8,128)} %reshape.118, bf16[2048,512]{1,0:T(8,128)(2,1)} %param.24, bf16[48,2048]{1,0:T(8,128)(2,1)S(1)} %copy-done.8, f32[2048]{0:T(1024)} %param.20, f32[48]{0:T(128)S(1)} %add_rsqrt_fusion.2), kind=kOutput, calls=%fused_computation.15 | convolution fusion | flops 202506192 | bytes 4694400 | tf_op jit(solution)/shard_map/dot_general | solution.py:66
  26.8 0.7 add_rsqrt_fusion.1
  27.4 0.8 %fusion.7.normed_ref = bf16[48,2048]{1,0:T(8,128)(2,1)S(1)} fusion(bf16[48,2048]{1,0:T(8,128)(2,1)S(1)} %get-tuple-element.11.mixed_ref, f32[2048]{0:T(1024)} %param.29, f32[48]{0:T(128)S(1)} %add_rsqrt_fusion.1), kind=kLoop, calls=%fused_computation.17 | loop fusion | flops 393216 | bytes 401600 | tf_op jit(solution)/shard_map/convert_element_type | solution.py:68
  28.3 1.2 %copy-done.2 = bf16[1,2048,256]{2,1,0:T(8,128)(2,1)S(1)} copy-done((bf16[1,2048,256]{2,1,0:T(8,128)(2,1)S(1)}, bf16[1,2048,256]{2,1,0:T(8,128)(2,1)}, u32[]{:S(2)}) %copy-start.2) | copy-done | bytes 1048600
  29.5 1.2 %copy-done.3 = bf16[1,256,2048]{2,1,0:T(8,128)(2,1)S(1)} copy-done((bf16[1,256,2048]{2,1,0:T(8,128)(2,1)S(1)}, bf16[1,256,2048]{2,1,0:T(8,128)(2,1)}, u32[]{:S(2)}) %copy-start.3) | copy-done | bytes 1048600
  30.7 48.9 %shard_map.185 = bf16[48,2048]{1,0:T(8,128)(2,1)S(1)} custom-call(bf16[48,2048]{1,0:T(8,128)(2,1)S(1)} %fusion.7.normed_ref, bf16[48,2048]{1,0:T(8,128)(2,1)S(1)} %get-tuple-element.11.mixed_ref, s32[1,48]{1,0:T(1,128)S(1)} %bitcast.17, s32[2,48]{1,0:T(2,128)S(1)} %bitcast.15, f32[2,48]{1,0:T(2,128)S(1)} %bitcast.16, bf16[1,2048,256]{2,1,0:T(8,128)(2,1)S(1)} %copy-done.1, ...), custom_call_target="tpu_custom_call" | custom-call | tf_op jit(solution)/shard_map/pallas_call | solution.py:233
  79.6 0.7 copy.26
  (24 shorter events, 0.1 us)
Async XLA Ops:
  0.6 22.8 %copy-start = (bf16[512,2048]{1,0:T(8,128)(2,1)S(1)}, bf16[512,2048]{1,0:T(8,128)(2,1)}, u32[]{:S(2)}) copy-start(bf16[512,2048]{1,0:T(8,128)(2,1)} %param.28) | copy-start | bytes 6291460
  0.6 3.8 %copy-start.8 = (bf16[48,2048]{1,0:T(8,128)(2,1)S(1)}, bf16[48,2048]{1,0:T(8,128)(2,1)}, u32[]{:S(2)}) copy-start(bf16[48,2048]{1,0:T(8,128)(2,1)} %param.18) | copy-start | bytes 589828
  0.7 3.8 %copy-start.10 = (f32[2048]{0:T(1024)S(1)}, f32[2048]{0:T(1024)}, u32[]{:S(2)}) copy-start(f32[2048]{0:T(1024)} %param.20) | copy-start | bytes 24580
  0.7 3.6 %copy-start.12 = (s32[48]{0:T(128)S(1)}, s32[48]{0:T(128)}, u32[]{:S(2)}) copy-start(s32[48]{0:T(128)} %param.19) | copy-start | bytes 580
  6.7 1.6 %copy-start.9 = (bf16[2048,512]{1,0:T(8,128)(2,1)S(1)}, bf16[2048,512]{1,0:T(8,128)(2,1)}, u32[]{:S(2)}) copy-start(bf16[2048,512]{1,0:T(8,128)(2,1)} %param.23) | copy-start | bytes 6291460
  6.9 2.0 %copy-start.13 = (f32[8]{0:T(128)S(1)}, f32[8]{0:T(128)}, u32[]{:S(2)}) copy-start(f32[8]{0:T(128)} %param.25) | copy-start | bytes 100
  17.4 4.8 %copy-start.7 = (f32[48,8,64,64]{3,2,1,0:T(8,128)}, f32[48,8,64,64]{3,2,1,0:T(8,128)S(1)}, u32[]{:S(2)}) copy-start(f32[48,8,64,64]{3,2,1,0:T(8,128)S(1)} %multiply_add_fusion) | copy-start | bytes 18874372
  17.4 4.8 %copy-start.11 = (f32[512]{0:T(512)S(1)}, f32[512]{0:T(512)}, u32[]{:S(2)}) copy-start(f32[512]{0:T(512)} %param.27) | copy-start | bytes 6148
  23.4 4.8 %copy-start.1 = (bf16[1,2048,256]{2,1,0:T(8,128)(2,1)S(1)}, bf16[1,2048,256]{2,1,0:T(8,128)(2,1)}, u32[]{:S(2)}) copy-start(bf16[1,2048,256]{2,1,0:T(8,128)(2,1)} %gate_hbm.1) | copy-start | bytes 3145732
  23.4 4.8 %copy-start.4 = (s32[48,2]{0,1:T(2,128)S(1)}, s32[48,2]{0,1:T(2,128)}, u32[]{:S(2)}) copy-start(s32[48,2]{0,1:T(2,128)} %param.32) | copy-start | bytes 1156
  23.4 4.8 %copy-start.5 = (f32[48,2]{0,1:T(2,128)S(1)}, f32[48,2]{0,1:T(2,128)}, u32[]{:S(2)}) copy-start(f32[48,2]{0,1:T(2,128)} %param.30) | copy-start | bytes 1156
  23.4 4.8 %copy-start.6 = (s32[48]{0:T(128)S(1)}, s32[48]{0:T(128)}, u32[]{:S(2)}) copy-start(s32[48]{0:T(128)} %param.31) | copy-start | bytes 580
  28.3 1.2 %copy-start.2 = (bf16[1,2048,256]{2,1,0:T(8,128)(2,1)S(1)}, bf16[1,2048,256]{2,1,0:T(8,128)(2,1)}, u32[]{:S(2)}) copy-start(bf16[1,2048,256]{2,1,0:T(8,128)(2,1)} %up_hbm.1) | copy-start | bytes 3145732
  29.5 1.2 %copy-start.3 = (bf16[1,256,2048]{2,1,0:T(8,128)(2,1)S(1)}, bf16[1,256,2048]{2,1,0:T(8,128)(2,1)}, u32[]{:S(2)}) copy-start(bf16[1,256,2048]{2,1,0:T(8,128)(2,1)} %down_hbm.1) | copy-start | bytes 3145732

commit v2 on v1

v2 whole, which is shorter than its diff:
```python
import numpy as np

import jax
import jax.numpy as jnp
from jax import lax
from jax.experimental import pallas as pl
from jax.experimental.pallas import tpu as pltpu
from jax.sharding import PartitionSpec as P

MESH = pl.DeviceIdType.MESH
F32 = jnp.float32
BF16 = jnp.bfloat16
GROUP_SIZE = 32
PLANES = 4
CHUNKS = 2
STATE_BLOCK = 8
epsilon = 1e-06


FAR = (2, 1, 3, 0)


def digits(me):
    return me // 32, (me // 8) % 4, (me // 2) % 4, me % 2


def each_partner(me, sign, plane, action):
    z, y, x, c = digits(me)
    base = ((z + 4 + sign * FAR[plane]) % 4) * 32
    inner = [
        ((x + 4 + sign * FAR[i // 2]) % 4) * 2 + (c + 1 - i % 2) % 2 for i in range(8)
    ]

    def row(t, count):
        far = (2 + 3 * ((t * (t + 1)) // 2)) % 4
        start = base + ((y + 4 + sign * far) % 4) * 8
        for i in range(count):
            action(plane * 32 + t * 8 + i, start + inner[i])

    def step(t, carry):
        row(t, 8)
        return carry

    last = plane == PLANES - 1
    lax.fori_loop(0, 3 if last else 4, step, 0)
    if last:
        row(3, 7)


def slot_experts(me, r):
    z, y, x, c = digits(me)
    j = r >> 1

    def far(t):
        return (2 + 3 * ((t * (t + 1)) >> 1)) & 3

    return (
        ((z + far(j >> 5)) & 3) * 32
        + ((y + far((j >> 3) & 3)) & 3) * 8
        + ((x + far((j >> 1) & 3)) & 3) * 2
        + ((c + 1 - (j & 1)) & 1)
    )


def rms_scale(values, gains):
    return values * lax.rsqrt(jnp.mean(values * values, axis=-1, keepdims=True) + epsilon) * gains


def layer_kernel(
    tokens_hbm, places_hbm, norm_gain_hbm, query_hbm, key_hbm, value_hbm, gating_hbm, decay_hbm,
    state_hbm, head_gain_hbm, out_hbm, moe_gain_hbm, route_hbm, group_hbm, inner_hbm, gate_hbm,
    up_hbm, down_hbm, inverse_hbm,
    out_ref, state,
    tokens, places, norm_gain, decay, head_gain, moe_gain, route, group, inner, inverse,
    w_query, w_key, w_value, w_gating, w_out, w_gate, w_up, w_down,
    keys_t, queries_t, values_h, decay_h, reading,
    token_out, token_in, mixed_out, mixed_in, results, returned,
    small_sems, weight_sems, state_sems,
    send_tok, recv_tok, send_mix, recv_mix, send_res, recv_res,
):
    me = lax.axis_index("ep")
    rows, width = tokens.shape
    heads, head_width = values_h.shape[1:]
    n = token_out.shape[0]
    slots = 2 * n
    plane_slots = n // PLANES
    per = n // CHUNKS
    blocks = rows // STATE_BLOCK

    def start(source, target, sem):
        copy = pltpu.make_async_copy(source, target, sem)
        copy.start()
        return copy

    smalls = [
        start(s, t, small_sems.at[i])
        for i, (s, t) in enumerate(
            (
                (group_hbm, group), (inner_hbm, inner), (tokens_hbm, tokens),
                (norm_gain_hbm, norm_gain), (places_hbm, places), (inverse_hbm, inverse),
                (decay_hbm, decay), (head_gain_hbm, head_gain), (moe_gain_hbm, moe_gain),
                (route_hbm, route),
            )
        )
    ]
    weights = [
        start(s, t, weight_sems.at[i])
        for i, (s, t) in enumerate(
            ((key_hbm, w_key), (query_hbm, w_query), (value_hbm, w_value), (gating_hbm, w_gating))
        )
    ]
    barrier = pltpu.get_barrier_semaphore()

    def greet(slot, device):
        pl.semaphore_signal(barrier, inc=1, device_id=(device,), device_id_type=MESH)

    for plane in range(PLANES):
        each_partner(me, 1, plane, greet)
    loads = [
        start(
            state_hbm.at[pl.ds(i * STATE_BLOCK, STATE_BLOCK)],
            state.at[pl.ds(i * STATE_BLOCK, STATE_BLOCK)],
            state_sems.at[i],
        )
        for i in range(blocks)
    ]
    weights += [
        start(s, t, weight_sems.at[4 + i])
        for i, (s, t) in enumerate(
            (
                (out_hbm, w_out), (gate_hbm.at[0], w_gate), (up_hbm.at[0], w_up),
                (down_hbm.at[0], w_down),
            )
        )
    ]
    for copy in smalls:
        copy.wait()

    first_row = group[...] * GROUP_SIZE + inner[0:1, :]
    second_row = group[...] * GROUP_SIZE + inner[1:2, :]
    sub = lax.broadcasted_iota(jnp.int32, (rows, rows), 0)
    lane = lax.broadcasted_iota(jnp.int32, (rows, rows), 1)

    def column(row):
        return jnp.sum(jnp.where(sub == lane, row, jnp.zeros_like(row)), axis=1, keepdims=True)

    first_col, second_col = column(first_row), column(second_row)

    def rank(ids_row):
        same = (first_col == ids_row).astype(F32) + (second_col == ids_row).astype(F32)
        return jnp.sum(jnp.where(sub < lane, same, 0.0), axis=0, keepdims=True)

    first_rank, second_rank = rank(first_row), rank(second_row)
    r_col = lax.broadcasted_iota(jnp.int32, (slots, 1), 0)
    expert_col = slot_experts(me, r_col)
    k_col = (r_col & 1).astype(F32)
    place = ((expert_col == first_row) & (k_col == first_rank)) | (
        (expert_col == second_row) & (k_col == second_rank)
    )
    place = place.astype(F32).astype(BF16)
    token_out[...] = (
        jnp.dot(place, tokens[...], preferred_element_type=F32).astype(BF16).reshape(n, 2, width)
    )
    inputs = tokens[...].astype(F32)
    normed = rms_scale(inputs, norm_gain[...]).astype(BF16)
    angles = column(places[...].astype(F32)) * inverse[...]
    cosine = jnp.concatenate([jnp.cos(angles)] * 4, axis=1)
    sine = jnp.concatenate([jnp.sin(angles)] * 4, axis=1)
    pl.semaphore_wait(barrier, n - 1)

    def remote(source, target, send_sem, recv_sems):
        def action(slot, device):
            pltpu.make_async_remote_copy(
                src_ref=source.at[slot], dst_ref=target.at[slot], send_sem=send_sem,
                recv_sem=recv_sems, device_id=(device,), device_id_type=MESH,
            ).start()

        return action

    for plane in range(PLANES):
        chunk = plane * CHUNKS // PLANES
        each_partner(me, 1, plane, remote(token_out, token_in, send_tok, recv_tok.at[chunk]))
    token_in[n - 1] = token_out[n - 1]

    def project(index, weight):
        weights[index].wait()
        return jnp.dot(normed, weight[...], preferred_element_type=F32).astype(BF16).astype(F32)

    first_half = (lax.broadcasted_iota(jnp.int32, (1, heads * head_width), 1) % head_width) < (
        head_width // 2
    )

    def rotate(x):
        total = heads * head_width
        half = head_width // 2
        swapped = jnp.where(first_half, -pltpu.roll(x, total - half, 1), pltpu.roll(x, half, 1))
        return x * cosine + swapped * sine

    def transposed(x):
        pad = jnp.zeros((128 - rows, x.shape[1]), F32)
        return jnp.concatenate([x, pad], axis=0).T

    keys_t[...] = transposed(rotate(project(0, w_key)) * head_width ** (-0.5))
    queries_t[...] = transposed(rotate(project(1, w_query)))
    values_h[...] = project(2, w_value).reshape(rows, heads, head_width)
    gating = project(3, w_gating)
    retain = jnp.exp(-decay[...])
    decay_h[...] = jnp.concatenate(
        [jnp.broadcast_to(retain[:, h : h + 1], (1, head_width)) for h in range(heads)], axis=0
    )

    def sequence(s, carry):
        index = jnp.full((head_width, 128), s, jnp.int32)
        for h in range(heads):
            part = pl.ds(h * head_width, head_width)

            def spread(ref):
                picked = jnp.take_along_axis(ref[part], index, axis=1, mode="promise_in_bounds")
                return picked[:, :head_width]

            new = decay_h[h : h + 1] * state[s, h] + spread(keys_t) * values_h[s, h : h + 1]
            state[s, h] = new
            reading[s, h : h + 1] = jnp.sum(spread(queries_t) * new, axis=0, keepdims=True)
        return carry

    for i in range(blocks):
        loads[i].wait()
        lax.fori_loop(i * STATE_BLOCK, (i + 1) * STATE_BLOCK, sequence, 0)

    read = reading[...]
    read = read * lax.rsqrt(jnp.mean(read * read, axis=-1, keepdims=True) + epsilon)
    read = read.reshape(rows, heads * head_width) * head_gain[...]
    mixed = (read * (gating * jax.nn.sigmoid(gating))).astype(BF16)
    mixed_out[...] = (
        jnp.dot(place, mixed, preferred_element_type=F32)
        .astype(BF16)
        .reshape(n, 2, mixed.shape[1])
    )
    for plane in range(PLANES):
        chunk = plane * CHUNKS // PLANES
        each_partner(me, 1, plane, remote(mixed_out, mixed_in, send_mix, recv_mix.at[chunk]))
    mixed_in[n - 1] = mixed_out[n - 1]
    weights[4].wait()

    def mix(rows_in, mixed_rows):
        added = jnp.dot(mixed_rows, w_out[...], preferred_element_type=F32)
        return (rows_in.astype(F32) + added).astype(BF16).astype(F32)

    own_tokens = mix(tokens[...], mixed)
    for copy in weights[5:]:
        copy.wait()

    r_row = lax.broadcasted_iota(jnp.int32, (1, slots), 1)
    expert_row = slot_experts(me, r_row)
    k_row = (r_row & 1).astype(F32)
    route_one, route_two = column(route[0:1, :]), column(route[1:2, :])
    first_k, second_k = column(first_rank), column(second_rank)
    scale = jnp.where(
        (first_col == expert_row) & (first_k == k_row), route_one, 0.0
    ) + jnp.where((second_col == expert_row) & (second_k == k_row), route_two, 0.0)
    high = scale.astype(BF16)
    low = (scale - high.astype(F32)).astype(BF16)

    def wait_block(ref, sem, begin, count):
        block = ref.at[pl.ds(begin, count)]
        pltpu.make_async_copy(block, block, sem).wait()

    for chunk in range(CHUNKS):
        begin = chunk * per
        count = per if chunk < CHUNKS - 1 else per - 1
        wait_block(token_in, recv_tok.at[chunk], begin, count)
        wait_block(mixed_in, recv_mix.at[chunk], begin, count)
        x = mix(
            token_in[pl.ds(begin, per)].reshape(2 * per, width),
            mixed_in[pl.ds(begin, per)].reshape(2 * per, mixed.shape[1]),
        )
        x = rms_scale(x, moe_gain[...]).astype(BF16)
        gate_part = jnp.dot(x, w_gate[...], preferred_element_type=F32)
        up_part = jnp.dot(x, w_up[...], preferred_element_type=F32)
        hidden = (gate_part * jax.nn.sigmoid(gate_part) * up_part).astype(BF16)
        y = jnp.dot(hidden, w_down[...], preferred_element_type=F32).astype(BF16)
        results[pl.ds(begin, per)] = y.reshape(per, 2, width)
        for plane in range(chunk * PLANES // CHUNKS, (chunk + 1) * PLANES // CHUNKS):
            each_partner(me, -1, plane, remote(results, returned, send_res, recv_res))
    returned[n - 1] = results[n - 1]

    wait_block(returned, recv_res, 0, n - 1)
    back = returned[...].reshape(slots, width)
    routed = jnp.dot(high, back, preferred_element_type=F32) + jnp.dot(
        low, back, preferred_element_type=F32
    )
    out_ref[...] = (own_tokens + routed).astype(BF16)
    wait_block(token_out, send_tok, 0, n - 1)
    wait_block(mixed_out, send_mix, 0, n - 1)
    wait_block(results, send_res, 0, n - 1)


def local(
    tokens, history_length, norm_gain, w_query, w_key, w_value, w_gate, decay_rate, state,
    head_gain, w_out, moe_gain, route_weights, expert_group, expert_inner, expert_gate,
    expert_up, expert_down,
):
    n = lax.axis_size("ep")
    rows, width = tokens.shape
    heads, head_width = state.shape[1], state.shape[2]
    ret_width = w_query.shape[1]
    hidden = expert_gate.shape[2]
    half = head_width // 2
    inverse = 10000.0 ** (-(np.arange(128) % half).astype(np.float64) / half)
    inverse = jnp.asarray(inverse.astype(np.float32)[None])
    operands = (
        tokens, history_length.reshape(1, rows), norm_gain.reshape(1, width), w_query, w_key,
        w_value, w_gate, decay_rate.reshape(1, heads), state, head_gain.reshape(1, ret_width),
        w_out, moe_gain.reshape(1, width), route_weights.T, expert_group.reshape(1, rows),
        expert_inner.T, expert_gate, expert_up, expert_down, inverse,
    )
    vmem = pl.BlockSpec(memory_space=pltpu.VMEM)
    hbm = pl.BlockSpec(memory_space=pltpu.HBM)
    V = pltpu.VMEM
    DMA = pltpu.SemaphoreType.DMA
    output, new_state = pl.pallas_call(
        layer_kernel,
        out_shape=(jax.ShapeDtypeStruct((rows, width), BF16), V(state.shape, F32)),
        in_specs=[hbm] * len(operands),
        out_specs=(vmem, vmem),
        scratch_shapes=[
            V((rows, width), BF16), V((1, rows), jnp.int32), V((1, width), F32),
            V((1, heads), F32), V((1, ret_width), F32), V((1, width), F32),
            V((2, rows), F32), V((1, rows), jnp.int32), V((2, rows), jnp.int32), V((1, 128), F32),
            V((width, ret_width), BF16), V((width, ret_width), BF16),
            V((width, ret_width), BF16), V((width, ret_width), BF16),
            V((ret_width, width), BF16), V((width, hidden), BF16), V((width, hidden), BF16),
            V((hidden, width), BF16),
            V((ret_width, 128), F32), V((ret_width, 128), F32), V((rows, heads, head_width), F32),
            V((heads, head_width), F32), V((rows, heads, head_width), F32),
            V((n, 2, width), BF16), V((n, 2, width), BF16),
            V((n, 2, ret_width), BF16), V((n, 2, ret_width), BF16),
            V((n, 2, width), BF16), V((n, 2, width), BF16),
            DMA((10,)), DMA((8,)), DMA((rows // STATE_BLOCK,)),
            DMA, DMA((CHUNKS,)), DMA, DMA((CHUNKS,)), DMA, DMA,
        ],
        compiler_params=pltpu.CompilerParams(
            collective_id=0, has_side_effects=True, vmem_limit_bytes=46 * 1024 * 1024
        ),
    )(*operands)
    return (output, new_state)


def solution(mesh):
    return jax.shard_map(
        local,
        mesh=mesh,
        in_specs=(
            P("ep", None), P("ep"), P(), P(), P(), P(), P(), P(), P("ep", None, None, None),
            P(), P(), P(), P("ep", None), P("ep"), P("ep", None), P("ep", None, None),
            P("ep", None, None), P("ep", None, None),
        ),
        out_specs=(P("ep", None), P("ep", None, None, None)),
        check_vma=False,
    )
```

time: 80.7 us -> 54.8 us (0.68)
  other arithmetic: 12 us -> 0 us
  matrix products: 9.95 us -> 0 us
  local copies, waits for them, and re-layouts: 8.57 us -> 5.46 us
    dot_general x5 -> x0, matrix products: 9.95 us -> none  [the longest x3 4.85 us: project(): jnp.dot(normed, weights, preferred_element_type=jnp.float32)]
    add x1 -> x0, other arithmetic: 8.47 us -> none  [retention_step(): retain[None, :, None, None] * state]
    unnamed x29 -> x4, local copies, waits for them, and re-layouts: 7.32 us -> 5.46 us
    reduce_sum x2 -> x0, other arithmetic: 1.34 us -> none  [rms_scale(): jnp.mean(values * values, axis=-1, keepdims=True) + epsilon]
    convert_element_type x2 -> x0, other arithmetic: 0.82 us -> none  [the longest x1 0.82 us: retention_step(): rms_scale(mixed_tokens.astype(jnp.float32), moe_gain).astype(jnp.bfloat16)]
where the time goes in v2:
time: 54.8 us; the launch traced here: 54.6 us
  Pallas kernels  48.5 us (89%)
  local copies, waits for them, and re-layouts  5.46 us (10%)
  between operations  0.65 us (1%)
    pallas_call x1, Pallas kernels, local(): pl.pallas_call(layer_kernel, out_shape=(jax.ShapeDtypeStruct((rows, width...  48.5 us
    unnamed x4, local copies, waits for them, and re-layouts  5.46 us

profile of v2, /device:TPU:1, one launch (start us, length us, event | category | flops | bytes accessed | tf_op | source)
XLA Modules:
  0.0 54.6 jit_solution(14641320659540712521)
XLA Ops:
  0.6 48.5 %shard_map.194 = (bf16[48,2048]{1,0:T(8,128)(2,1)}, f32[48,8,64,64]{3,2,1,0:T(8,128)S(1)}) custom-call(bf16[48,2048]{1,0:T(8,128)(2,1)} %tokens_hbm.1, s32[1,48]{1,0:T(1,128)} %bitcast.13, f32[1,2048]{1,0:T(1,128)} %bitcast.8, bf16[2048,512]{1,0:T(8,128)(2,1)} %query_hbm.1, bf16[2048,512]{1,0:T(8,128)(2,1)} %key_hbm.1, bf16[2048,512]{1,0:T(8,128)(2,1)} %value_hbm.1, ...), custom_call_target="tpu_custom_call" | custom-call | tf_op jit(solution)/shard_map/pallas_call | solution.py:321
  49.2 0.0 copy-start
  49.2 4.8 %copy.23 = f32[48,8,64,64]{3,2,1,0:T(8,128)} copy(f32[48,8,64,64]{3,2,1,0:T(8,128)S(1)} %get-tuple-element.3) | data formatting | bytes 12582912
  54.0 0.0 copy-done
  54.0 0.7 %copy.24 = bf16[48,2048]{1,0:T(8,128)(2,1)} copy(bf16[48,2048]{1,0:T(8,128)(2,1)S(1)} %copy-done) | data formatting | bytes 393216
Async XLA Ops:
  49.2 4.8 %copy-start = (bf16[48,2048]{1,0:T(8,128)(2,1)S(1)}, bf16[48,2048]{1,0:T(8,128)(2,1)}, u32[]{:S(2)}) copy-start(bf16[48,2048]{1,0:T(8,128)(2,1)} %get-tuple-element.6) | copy-start | bytes 589828

commit v3 on v2

--- a/solution.py
+++ b/solution.py
@@ -12,7 +12,7 @@
 BF16 = jnp.bfloat16
 GROUP_SIZE = 32
 PLANES = 4
-CHUNKS = 2
+CHUNKS = 4
 STATE_BLOCK = 8
 epsilon = 1e-06
 
@@ -73,7 +73,7 @@
     out_ref, state,
     tokens, places, norm_gain, decay, head_gain, moe_gain, route, group, inner, inverse,
     w_query, w_key, w_value, w_gating, w_out, w_gate, w_up, w_down,
-    keys_t, queries_t, values_h, decay_h, reading,
+    keys_t, queries, values_h, decay_h, reading,
     token_out, token_in, mixed_out, mixed_in, results, returned,
     small_sems, weight_sems, state_sems,
     send_tok, recv_tok, send_mix, recv_mix, send_res, recv_res,
@@ -201,7 +201,14 @@
         return jnp.concatenate([x, pad], axis=0).T
 
     keys_t[...] = transposed(rotate(project(0, w_key)) * head_width ** (-0.5))
-    queries_t[...] = transposed(rotate(project(1, w_query)))
+    query = rotate(project(1, w_query))
+    query_high = query.astype(BF16).astype(F32)
+    head_of = lax.broadcasted_iota(jnp.int32, (1, heads, heads * head_width), 2) // head_width
+    head_row = lax.broadcasted_iota(jnp.int32, (1, heads, heads * head_width), 1)
+    for i, piece in enumerate((query_high, query - query_high)):
+        queries[:, pl.ds(i * heads, heads)] = jnp.where(
+            head_of == head_row, piece[:, None, :], 0.0
+        ).astype(BF16)
     values_h[...] = project(2, w_value).reshape(rows, heads, head_width)
     gating = project(3, w_gating)
     retain = jnp.exp(-decay[...])
@@ -211,21 +218,25 @@
 
     def sequence(s, carry):
         index = jnp.full((head_width, 128), s, jnp.int32)
+        rounded = []
         for h in range(heads):
-            part = pl.ds(h * head_width, head_width)
-
-            def spread(ref):
-                picked = jnp.take_along_axis(ref[part], index, axis=1, mode="promise_in_bounds")
-                return picked[:, :head_width]
-
-            new = decay_h[h : h + 1] * state[s, h] + spread(keys_t) * values_h[s, h : h + 1]
+            key = jnp.take_along_axis(
+                keys_t[pl.ds(h * head_width, head_width)], index, axis=1, mode="promise_in_bounds"
+            )[:, :head_width]
+            new = decay_h[h : h + 1] * state[s, h] + key * values_h[s, h : h + 1]
             state[s, h] = new
-            reading[s, h : h + 1] = jnp.sum(spread(queries_t) * new, axis=0, keepdims=True)
+            rounded.append(new.astype(BF16))
+        read = jnp.dot(
+            queries[s], jnp.concatenate(rounded, axis=0), preferred_element_type=F32
+        )
+        reading[s] = read[:heads] + read[heads:]
         return carry
 
     for i in range(blocks):
         loads[i].wait()
-        lax.fori_loop(i * STATE_BLOCK, (i + 1) * STATE_BLOCK, sequence, 0)
+        lax.fori_loop(
+            i * STATE_BLOCK, (i + 1) * STATE_BLOCK, sequence, 0, unroll=STATE_BLOCK
+        )
 
     read = reading[...]
     read = read * lax.rsqrt(jnp.mean(read * read, axis=-1, keepdims=True) + epsilon)
@@ -293,6 +304,22 @@
     wait_block(token_out, send_tok, 0, n - 1)
     wait_block(mixed_out, send_mix, 0, n - 1)
     wait_block(results, send_res, 0, n - 1)
+
+
+def write_kernel(output, new_state, output_hbm, state_hbm, sems):
+    pieces = sems.shape[0] - 1
+    size = new_state.shape[0] // pieces
+    copies = [
+        pltpu.make_async_copy(
+            new_state.at[pl.ds(i * size, size)], state_hbm.at[pl.ds(i * size, size)], sems.at[i]
+        )
+        for i in range(pieces)
+    ]
+    copies.append(pltpu.make_async_copy(output, output_hbm, sems.at[pieces]))
+    for copy in copies:
+        copy.start()
+    for copy in copies:
+        copy.wait()
 
 
 def local(
@@ -320,7 +347,7 @@
     DMA = pltpu.SemaphoreType.DMA
     output, new_state = pl.pallas_call(
         layer_kernel,
-        out_shape=(jax.ShapeDtypeStruct((rows, width), BF16), V(state.shape, F32)),
+        out_shape=(V((rows, width), BF16), V(state.shape, F32)),
         in_specs=[hbm] * len(operands),
         out_specs=(vmem, vmem),
         scratch_shapes=[
@@ -331,7 +358,8 @@
             V((width, ret_width), BF16), V((width, ret_width), BF16),
             V((ret_width, width), BF16), V((width, hidden), BF16), V((width, hidden), BF16),
             V((hidden, width), BF16),
-            V((ret_width, 128), F32), V((ret_width, 128), F32), V((rows, heads, head_width), F32),
+            V((ret_width, 128), F32), V((rows, 2 * heads, ret_width), BF16),
+            V((rows, heads, head_width), F32),
             V((heads, head_width), F32), V((rows, heads, head_width), F32),
             V((n, 2, width), BF16), V((n, 2, width), BF16),
             V((n, 2, ret_width), BF16), V((n, 2, ret_width), BF16),
@@ -343,7 +371,20 @@
             collective_id=0, has_side_effects=True, vmem_limit_bytes=46 * 1024 * 1024
         ),
     )(*operands)
-    return (output, new_state)
+    pieces = 8
+    return pl.pallas_call(
+        write_kernel,
+        out_shape=(
+            jax.ShapeDtypeStruct((rows, width), BF16), jax.ShapeDtypeStruct(state.shape, F32),
+        ),
+        in_specs=[vmem, vmem],
+        out_specs=(hbm, hbm),
+        scratch_shapes=[DMA((pieces + 1,))],
+        compiler_params=pltpu.CompilerParams(vmem_limit_bytes=1024 * 1024),
+    )(
+        pltpu.with_memory_space_constraint(output, pltpu.VMEM),
+        pltpu.with_memory_space_constraint(new_state, pltpu.VMEM),
+    )
 
 
 def solution(mesh):

time: 54.8 us -> 52 us (0.949)
  local copies, waits for them, and re-layouts: 5.46 us -> 0 us
  Pallas kernels: 48.5 us -> 51.3 us
    unnamed x4 -> x0, local copies, waits for them, and re-layouts: 5.46 us -> none
    pallas_call x1 -> x2, Pallas kernels: 48.5 us -> 51.3 us  [the longest x1 46.6 us: local(): pl.pallas_call(layer_kernel, out_shape=(V((rows, width), BF16), V(state.s...]
where the time goes in v3:
time: 52 us; the launch traced here: 51.9 us
  Pallas kernels  51.3 us (99%)
  between operations  0.65 us (1%)
    pallas_call x1, Pallas kernels, local(): pl.pallas_call(layer_kernel, out_shape=(V((rows, width), BF16), V(state.s...  46.6 us
    pallas_call x1, Pallas kernels, local(): pl.pallas_call(write_kernel, out_shape=(jax.ShapeDtypeStruct((rows, width...  4.68 us

profile of v3, /device:TPU:1, one launch (start us, length us, event | category | flops | bytes accessed | tf_op | source)
XLA Modules:
  0.0 51.9 jit_solution(18018509494744876210)
XLA Ops:
  0.6 46.6 %shard_map.194 = (bf16[48,2048]{1,0:T(8,128)(2,1)S(1)}, f32[48,8,64,64]{3,2,1,0:T(8,128)S(1)}) custom-call(bf16[48,2048]{1,0:T(8,128)(2,1)} %tokens_hbm.1, s32[1,48]{1,0:T(1,128)} %bitcast.13, f32[1,2048]{1,0:T(1,128)} %bitcast.8, bf16[2048,512]{1,0:T(8,128)(2,1)} %query_hbm.1, bf16[2048,512]{1,0:T(8,128)(2,1)} %key_hbm.1, bf16[2048,512]{1,0:T(8,128)(2,1)} %value_hbm.1, ...), custom_call_target="tpu_custom_call" | custom-call | tf_op jit(solution)/shard_map/pallas_call | solution.py:348
  47.2 4.7 %shard_map.195 = (bf16[48,2048]{1,0:T(8,128)(2,1)}, f32[48,8,64,64]{3,2,1,0:T(8,128)}) custom-call(bf16[48,2048]{1,0:T(8,128)(2,1)S(1)} %get-tuple-element.4.output, f32[48,8,64,64]{3,2,1,0:T(8,128)S(1)} %get-tuple-element.5.new_state), custom_call_target="tpu_custom_call" | custom-call | tf_op jit(solution)/shard_map/pallas_call | solution.py:375

commit v4 on v3

--- a/solution.py
+++ b/solution.py
@@ -12,7 +12,7 @@
 BF16 = jnp.bfloat16
 GROUP_SIZE = 32
 PLANES = 4
-CHUNKS = 4
+EARLY = 2
 STATE_BLOCK = 8
 epsilon = 1e-06
 
@@ -26,25 +26,15 @@
 
 def each_partner(me, sign, plane, action):
     z, y, x, c = digits(me)
-    base = ((z + 4 + sign * FAR[plane]) % 4) * 32
+    planes = [((z + 4 + sign * far) % 4) * 32 for far in FAR]
+    lines = [((y + 4 + sign * far) % 4) * 8 for far in FAR]
     inner = [
         ((x + 4 + sign * FAR[i // 2]) % 4) * 2 + (c + 1 - i % 2) % 2 for i in range(8)
     ]
-
-    def row(t, count):
-        far = (2 + 3 * ((t * (t + 1)) // 2)) % 4
-        start = base + ((y + 4 + sign * far) % 4) * 8
-        for i in range(count):
-            action(plane * 32 + t * 8 + i, start + inner[i])
-
-    def step(t, carry):
-        row(t, 8)
-        return carry
-
-    last = plane == PLANES - 1
-    lax.fori_loop(0, 3 if last else 4, step, 0)
-    if last:
-        row(3, 7)
+    for i in range(31 if plane == PLANES - 1 else 32):
+        t = i // 8
+        offset = (plane + 2 - t - (i % 8) // 2) % 4
+        action(plane * 32 + i, planes[offset] + lines[t] + inner[i % 8])
 
 
 def slot_experts(me, r):
@@ -55,7 +45,7 @@
         return (2 + 3 * ((t * (t + 1)) >> 1)) & 3
 
     return (
-        ((z + far(j >> 5)) & 3) * 32
+        ((z + far(((j >> 5) + 2 - (j >> 3) - (j >> 1)) & 3)) & 3) * 32
         + ((y + far((j >> 3) & 3)) & 3) * 8
         + ((x + far((j >> 1) & 3)) & 3) * 2
         + ((c + 1 - (j & 1)) & 1)
@@ -83,8 +73,8 @@
     heads, head_width = values_h.shape[1:]
     n = token_out.shape[0]
     slots = 2 * n
-    plane_slots = n // PLANES
-    per = n // CHUNKS
+    per = n // PLANES
+    early = EARLY * per
     blocks = rows // STATE_BLOCK
 
     def start(source, target, sem):
@@ -158,15 +148,17 @@
         (expert_col == second_row) & (k_col == second_rank)
     )
     place = place.astype(F32).astype(BF16)
-    token_out[...] = (
-        jnp.dot(place, tokens[...], preferred_element_type=F32).astype(BF16).reshape(n, 2, width)
-    )
+
+    def slab(chosen, values):
+        taken = jnp.dot(chosen, values, preferred_element_type=F32).astype(BF16)
+        return taken.reshape(chosen.shape[0] // 2, 2, values.shape[1])
+
+    token_out[pl.ds(0, early)] = slab(place[: 2 * early], tokens[...])
     inputs = tokens[...].astype(F32)
     normed = rms_scale(inputs, norm_gain[...]).astype(BF16)
     angles = column(places[...].astype(F32)) * inverse[...]
     cosine = jnp.concatenate([jnp.cos(angles)] * 4, axis=1)
     sine = jnp.concatenate([jnp.sin(angles)] * 4, axis=1)
-    pl.semaphore_wait(barrier, n - 1)
 
     def remote(source, target, send_sem, recv_sems):
         def action(slot, device):
@@ -177,10 +169,6 @@
 
         return action
 
-    for plane in range(PLANES):
-        chunk = plane * CHUNKS // PLANES
-        each_partner(me, 1, plane, remote(token_out, token_in, send_tok, recv_tok.at[chunk]))
-    token_in[n - 1] = token_out[n - 1]
 
     def project(index, weight):
         weights[index].wait()
@@ -232,6 +220,10 @@
         reading[s] = read[:heads] + read[heads:]
         return carry
 
+    pl.semaphore_wait(barrier, n - 1)
+    for plane in range(EARLY):
+        each_partner(me, 1, plane, remote(token_out, token_in, send_tok, recv_tok.at[plane]))
+
     for i in range(blocks):
         loads[i].wait()
         lax.fori_loop(
@@ -242,15 +234,9 @@
     read = read * lax.rsqrt(jnp.mean(read * read, axis=-1, keepdims=True) + epsilon)
     read = read.reshape(rows, heads * head_width) * head_gain[...]
     mixed = (read * (gating * jax.nn.sigmoid(gating))).astype(BF16)
-    mixed_out[...] = (
-        jnp.dot(place, mixed, preferred_element_type=F32)
-        .astype(BF16)
-        .reshape(n, 2, mixed.shape[1])
-    )
-    for plane in range(PLANES):
-        chunk = plane * CHUNKS // PLANES
-        each_partner(me, 1, plane, remote(mixed_out, mixed_in, send_mix, recv_mix.at[chunk]))
-    mixed_in[n - 1] = mixed_out[n - 1]
+    mixed_out[pl.ds(0, early)] = slab(place[: 2 * early], mixed)
+    for plane in range(EARLY):
+        each_partner(me, 1, plane, remote(mixed_out, mixed_in, send_mix, recv_mix.at[plane]))
     weights[4].wait()
 
     def mix(rows_in, mixed_rows):
@@ -258,6 +244,11 @@
         return (rows_in.astype(F32) + added).astype(BF16).astype(F32)
 
     own_tokens = mix(tokens[...], mixed)
+    direct = rms_scale(own_tokens, moe_gain[...]).astype(BF16)
+    token_out[pl.ds(early, n - early)] = slab(place[2 * early :], direct)
+    for plane in range(EARLY, PLANES):
+        each_partner(me, 1, plane, remote(token_out, token_in, send_tok, recv_tok.at[plane]))
+    token_in[n - 1] = token_out[n - 1]
     for copy in weights[5:]:
         copy.wait()
 
@@ -276,23 +267,21 @@
         block = ref.at[pl.ds(begin, count)]
         pltpu.make_async_copy(block, block, sem).wait()
 
-    for chunk in range(CHUNKS):
-        begin = chunk * per
-        count = per if chunk < CHUNKS - 1 else per - 1
-        wait_block(token_in, recv_tok.at[chunk], begin, count)
-        wait_block(mixed_in, recv_mix.at[chunk], begin, count)
-        x = mix(
-            token_in[pl.ds(begin, per)].reshape(2 * per, width),
-            mixed_in[pl.ds(begin, per)].reshape(2 * per, mixed.shape[1]),
-        )
-        x = rms_scale(x, moe_gain[...]).astype(BF16)
+    for plane in range(PLANES):
+        begin = plane * per
+        count = per if plane < PLANES - 1 else per - 1
+        wait_block(token_in, recv_tok.at[plane], begin, count)
+        x = token_in[pl.ds(begin, per)].reshape(2 * per, width)
+        if plane < EARLY:
+            wait_block(mixed_in, recv_mix.at[plane], begin, count)
+            x = mix(x, mixed_in[pl.ds(begin, per)].reshape(2 * per, mixed.shape[1]))
+            x = rms_scale(x, moe_gain[...]).astype(BF16)
         gate_part = jnp.dot(x, w_gate[...], preferred_element_type=F32)
         up_part = jnp.dot(x, w_up[...], preferred_element_type=F32)
         hidden = (gate_part * jax.nn.sigmoid(gate_part) * up_part).astype(BF16)
         y = jnp.dot(hidden, w_down[...], preferred_element_type=F32).astype(BF16)
         results[pl.ds(begin, per)] = y.reshape(per, 2, width)
-        for plane in range(chunk * PLANES // CHUNKS, (chunk + 1) * PLANES // CHUNKS):
-            each_partner(me, -1, plane, remote(results, returned, send_res, recv_res))
+        each_partner(me, -1, plane, remote(results, returned, send_res, recv_res))
     returned[n - 1] = results[n - 1]
 
     wait_block(returned, recv_res, 0, n - 1)
@@ -302,7 +291,7 @@
     )
     out_ref[...] = (own_tokens + routed).astype(BF16)
     wait_block(token_out, send_tok, 0, n - 1)
-    wait_block(mixed_out, send_mix, 0, n - 1)
+    wait_block(mixed_out, send_mix, 0, early)
     wait_block(results, send_res, 0, n - 1)
 
 
@@ -365,7 +354,7 @@
             V((n, 2, ret_width), BF16), V((n, 2, ret_width), BF16),
             V((n, 2, width), BF16), V((n, 2, width), BF16),
             DMA((10,)), DMA((8,)), DMA((rows // STATE_BLOCK,)),
-            DMA, DMA((CHUNKS,)), DMA, DMA((CHUNKS,)), DMA, DMA,
+            DMA, DMA((PLANES,)), DMA, DMA((EARLY,)), DMA, DMA,
         ],
         compiler_params=pltpu.CompilerParams(
             collective_id=0, has_side_effects=True, vmem_limit_bytes=46 * 1024 * 1024

time: 52 us -> 45.1 us (0.87)
  Pallas kernels: 51.3 us -> 44.4 us
    pallas_call x1, Pallas kernels: 46.6 us -> 39.7 us  [local(): pl.pallas_call(layer_kernel, out_shape=(V((rows, width), BF16), V(state.s...]
where the time goes in v4:
time: 45.1 us; the launch traced here: 45 us
  Pallas kernels  44.4 us (98%)
  between operations  0.65 us (1%)
    pallas_call x1, Pallas kernels, local(): pl.pallas_call(layer_kernel, out_shape=(V((rows, width), BF16), V(state.s...  39.7 us
    pallas_call x1, Pallas kernels, local(): pl.pallas_call(write_kernel, out_shape=(jax.ShapeDtypeStruct((rows, width...  4.68 us

profile of v4, /device:TPU:1, one launch (start us, length us, event | category | flops | bytes accessed | tf_op | source)
XLA Modules:
  0.0 45.0 jit_solution(9887238760841084952)
XLA Ops:
  0.6 39.7 %shard_map.194 = (bf16[48,2048]{1,0:T(8,128)(2,1)S(1)}, f32[48,8,64,64]{3,2,1,0:T(8,128)S(1)}) custom-call(bf16[48,2048]{1,0:T(8,128)(2,1)} %tokens_hbm.1, s32[1,48]{1,0:T(1,128)} %bitcast.13, f32[1,2048]{1,0:T(1,128)} %bitcast.8, bf16[2048,512]{1,0:T(8,128)(2,1)} %query_hbm.1, bf16[2048,512]{1,0:T(8,128)(2,1)} %key_hbm.1, bf16[2048,512]{1,0:T(8,128)(2,1)} %value_hbm.1, ...), custom_call_target="tpu_custom_call" | custom-call | tf_op jit(solution)/shard_map/pallas_call | solution.py:337
  40.3 4.7 %shard_map.195 = (bf16[48,2048]{1,0:T(8,128)(2,1)}, f32[48,8,64,64]{3,2,1,0:T(8,128)}) custom-call(bf16[48,2048]{1,0:T(8,128)(2,1)S(1)} %get-tuple-element.4.output, f32[48,8,64,64]{3,2,1,0:T(8,128)S(1)} %get-tuple-element.5.new_state), custom_call_target="tpu_custom_call" | custom-call | tf_op jit(solution)/shard_map/pallas_call | solution.py:364

commit v5 on v4

--- a/solution.py
+++ b/solution.py
@@ -24,17 +24,27 @@
     return me // 32, (me // 8) % 4, (me // 2) % 4, me % 2
 
 
-def each_partner(me, sign, plane, action):
+def hops(plane, i):
+    t, u = i // 8, (i % 8) // 2
+    steps = [FAR[(plane + 2 - t - u) % 4], FAR[t], FAR[u]]
+    return sum(min(step, 4 - step) for step in steps)
+
+
+def chunk_order(plane):
+    return list(range(31 if plane == PLANES - 1 else 32))
+
+
+def each_partner(me, sign, plane, action, order=None):
     z, y, x, c = digits(me)
     planes = [((z + 4 + sign * far) % 4) * 32 for far in FAR]
     lines = [((y + 4 + sign * far) % 4) * 8 for far in FAR]
     inner = [
         ((x + 4 + sign * FAR[i // 2]) % 4) * 2 + (c + 1 - i % 2) % 2 for i in range(8)
     ]
-    for i in range(31 if plane == PLANES - 1 else 32):
+    for p, i in order or [(plane, i) for i in chunk_order(plane)]:
         t = i // 8
-        offset = (plane + 2 - t - (i % 8) // 2) % 4
-        action(plane * 32 + i, planes[offset] + lines[t] + inner[i % 8])
+        offset = (p + 2 - t - (i % 8) // 2) % 4
+        action(p * 32 + i, planes[offset] + lines[t] + inner[i % 8])
 
 
 def slot_experts(me, r):
@@ -93,19 +103,50 @@
             )
         )
     ]
+    barrier = pltpu.get_barrier_semaphore()
+
+    def greet(slot, device):
+        pl.semaphore_signal(barrier, inc=1, device_id=(device,), device_id_type=MESH)
+
+    everyone = [(p, i) for p in range(PLANES) for i in chunk_order(p)]
+    each_partner(me, 1, 0, greet, sorted(everyone, key=lambda pair: -hops(*pair)))
     weights = [
         start(s, t, weight_sems.at[i])
         for i, (s, t) in enumerate(
             ((key_hbm, w_key), (query_hbm, w_query), (value_hbm, w_value), (gating_hbm, w_gating))
         )
     ]
-    barrier = pltpu.get_barrier_semaphore()
-
-    def greet(slot, device):
-        pl.semaphore_signal(barrier, inc=1, device_id=(device,), device_id_type=MESH)
-
-    for plane in range(PLANES):
-        each_partner(me, 1, plane, greet)
+    for copy in smalls:
+        copy.wait()
+
+    first_row = group[...] * GROUP_SIZE + inner[0:1, :]
+    second_row = group[...] * GROUP_SIZE + inner[1:2, :]
+    sub = lax.broadcasted_iota(jnp.int32, (rows, rows), 0)
+    lane = lax.broadcasted_iota(jnp.int32, (rows, rows), 1)
+
+    def column(row):
+        return jnp.sum(jnp.where(sub == lane, row, jnp.zeros_like(row)), axis=1, keepdims=True)
+
+    first_col, second_col = column(first_row), column(second_row)
+
+    def rank(ids_row):
+        same = (first_col == ids_row).astype(F32) + (second_col == ids_row).astype(F32)
+        return jnp.sum(jnp.where(sub < lane, same, 0.0), axis=0, keepdims=True)
+
+    first_rank, second_rank = rank(first_row), rank(second_row)
+    r_col = lax.broadcasted_iota(jnp.int32, (slots, 1), 0)
+    expert_col = slot_experts(me, r_col)
+    k_col = (r_col & 1).astype(F32)
+    place = ((expert_col == first_row) & (k_col == first_rank)) | (
+        (expert_col == second_row) & (k_col == second_rank)
+    )
+    place = place.astype(F32).astype(BF16)
+
+    def slab(chosen, values):
+        taken = jnp.dot(chosen, values, preferred_element_type=F32).astype(BF16)
+        return taken.reshape(chosen.shape[0] // 2, 2, values.shape[1])
+
+    token_out[pl.ds(0, early)] = slab(place[: 2 * early], tokens[...])
     loads = [
         start(
             state_hbm.at[pl.ds(i * STATE_BLOCK, STATE_BLOCK)],
@@ -123,37 +164,6 @@
             )
         )
     ]
-    for copy in smalls:
-        copy.wait()
-
-    first_row = group[...] * GROUP_SIZE + inner[0:1, :]
-    second_row = group[...] * GROUP_SIZE + inner[1:2, :]
-    sub = lax.broadcasted_iota(jnp.int32, (rows, rows), 0)
-    lane = lax.broadcasted_iota(jnp.int32, (rows, rows), 1)
-
-    def column(row):
-        return jnp.sum(jnp.where(sub == lane, row, jnp.zeros_like(row)), axis=1, keepdims=True)
-
-    first_col, second_col = column(first_row), column(second_row)
-
-    def rank(ids_row):
-        same = (first_col == ids_row).astype(F32) + (second_col == ids_row).astype(F32)
-        return jnp.sum(jnp.where(sub < lane, same, 0.0), axis=0, keepdims=True)
-
-    first_rank, second_rank = rank(first_row), rank(second_row)
-    r_col = lax.broadcasted_iota(jnp.int32, (slots, 1), 0)
-    expert_col = slot_experts(me, r_col)
-    k_col = (r_col & 1).astype(F32)
-    place = ((expert_col == first_row) & (k_col == first_rank)) | (
-        (expert_col == second_row) & (k_col == second_rank)
-    )
-    place = place.astype(F32).astype(BF16)
-
-    def slab(chosen, values):
-        taken = jnp.dot(chosen, values, preferred_element_type=F32).astype(BF16)
-        return taken.reshape(chosen.shape[0] // 2, 2, values.shape[1])
-
-    token_out[pl.ds(0, early)] = slab(place[: 2 * early], tokens[...])
     inputs = tokens[...].astype(F32)
     normed = rms_scale(inputs, norm_gain[...]).astype(BF16)
     angles = column(places[...].astype(F32)) * inverse[...]

time: 45.1 us -> 44.3 us (0.982)
  Pallas kernels: 44.4 us -> 43.5 us
    pallas_call x1, Pallas kernels: 39.7 us -> 38.8 us  [local(): pl.pallas_call(layer_kernel, out_shape=(V((rows, width), BF16), V(state.s...]
where the time goes in v5:
time: 44.3 us; the launch traced here: 44.1 us
  Pallas kernels  43.5 us (98%)
  between operations  0.65 us (1%)
    pallas_call x1, Pallas kernels, local(): pl.pallas_call(layer_kernel, out_shape=(V((rows, width), BF16), V(state.s...  38.8 us
    pallas_call x1, Pallas kernels, local(): pl.pallas_call(write_kernel, out_shape=(jax.ShapeDtypeStruct((rows, width...  4.68 us

profile of v5, /device:TPU:1, one launch (start us, length us, event | category | flops | bytes accessed | tf_op | source)
XLA Modules:
  0.0 44.1 jit_solution(3431430111605803923)
XLA Ops:
  0.6 38.8 %shard_map.194 = (bf16[48,2048]{1,0:T(8,128)(2,1)S(1)}, f32[48,8,64,64]{3,2,1,0:T(8,128)S(1)}) custom-call(bf16[48,2048]{1,0:T(8,128)(2,1)} %tokens_hbm.1, s32[1,48]{1,0:T(1,128)} %bitcast.13, f32[1,2048]{1,0:T(1,128)} %bitcast.8, bf16[2048,512]{1,0:T(8,128)(2,1)} %query_hbm.1, bf16[2048,512]{1,0:T(8,128)(2,1)} %key_hbm.1, bf16[2048,512]{1,0:T(8,128)(2,1)} %value_hbm.1, ...), custom_call_target="tpu_custom_call" | custom-call | tf_op jit(solution)/shard_map/pallas_call | solution.py:347
  39.5 4.7 %shard_map.195 = (bf16[48,2048]{1,0:T(8,128)(2,1)}, f32[48,8,64,64]{3,2,1,0:T(8,128)}) custom-call(bf16[48,2048]{1,0:T(8,128)(2,1)S(1)} %get-tuple-element.4.output, f32[48,8,64,64]{3,2,1,0:T(8,128)S(1)} %get-tuple-element.5.new_state), custom_call_target="tpu_custom_call" | custom-call | tf_op jit(solution)/shard_map/pallas_call | solution.py:374

commit v6 on v5

--- a/solution.py
+++ b/solution.py
@@ -291,15 +291,20 @@
         hidden = (gate_part * jax.nn.sigmoid(gate_part) * up_part).astype(BF16)
         y = jnp.dot(hidden, w_down[...], preferred_element_type=F32).astype(BF16)
         results[pl.ds(begin, per)] = y.reshape(per, 2, width)
-        each_partner(me, -1, plane, remote(results, returned, send_res, recv_res))
+        each_partner(me, -1, plane, remote(results, returned, send_res, recv_res.at[plane]))
     returned[n - 1] = results[n - 1]
 
-    wait_block(returned, recv_res, 0, n - 1)
-    back = returned[...].reshape(slots, width)
-    routed = jnp.dot(high, back, preferred_element_type=F32) + jnp.dot(
-        low, back, preferred_element_type=F32
-    )
-    out_ref[...] = (own_tokens + routed).astype(BF16)
+    both = jnp.concatenate([high, low], axis=0)
+    routed = own_tokens
+    for plane in range(PLANES):
+        begin = plane * per
+        wait_block(returned, recv_res.at[plane], begin, per if plane < PLANES - 1 else per - 1)
+        back = returned[pl.ds(begin, per)].reshape(2 * per, width)
+        parts = jnp.dot(
+            both[:, 2 * begin : 2 * (begin + per)], back, preferred_element_type=F32
+        )
+        routed = routed + parts[:rows] + parts[rows:]
+    out_ref[...] = routed.astype(BF16)
     wait_block(token_out, send_tok, 0, n - 1)
     wait_block(mixed_out, send_mix, 0, early)
     wait_block(results, send_res, 0, n - 1)
@@ -364,7 +369,7 @@
             V((n, 2, ret_width), BF16), V((n, 2, ret_width), BF16),
             V((n, 2, width), BF16), V((n, 2, width), BF16),
             DMA((10,)), DMA((8,)), DMA((rows // STATE_BLOCK,)),
-            DMA, DMA((PLANES,)), DMA, DMA((EARLY,)), DMA, DMA,
+            DMA, DMA((PLANES,)), DMA, DMA((EARLY,)), DMA, DMA((PLANES,)),
         ],
         compiler_params=pltpu.CompilerParams(
             collective_id=0, has_side_effects=True, vmem_limit_bytes=46 * 1024 * 1024

time: 44.3 us -> 44.2 us (level)
  no operation moved by 1% of the time
where the time goes in v6:
time: 44.2 us; the launch traced here: 44.1 us
  Pallas kernels  43.4 us (98%)
  between operations  0.65 us (1%)
    pallas_call x1, Pallas kernels, local(): pl.pallas_call(layer_kernel, out_shape=(V((rows, width), BF16), V(state.s...  38.8 us
    pallas_call x1, Pallas kernels, local(): pl.pallas_call(write_kernel, out_shape=(jax.ShapeDtypeStruct((rows, width...  4.68 us

profile of v6, /device:TPU:1, one launch (start us, length us, event | category | flops | bytes accessed | tf_op | source)
XLA Modules:
  0.0 44.1 jit_solution(12219646475731063913)
XLA Ops:
  0.6 38.8 %shard_map.194 = (bf16[48,2048]{1,0:T(8,128)(2,1)S(1)}, f32[48,8,64,64]{3,2,1,0:T(8,128)S(1)}) custom-call(bf16[48,2048]{1,0:T(8,128)(2,1)} %tokens_hbm.1, s32[1,48]{1,0:T(1,128)} %bitcast.13, f32[1,2048]{1,0:T(1,128)} %bitcast.8, bf16[2048,512]{1,0:T(8,128)(2,1)} %query_hbm.1, bf16[2048,512]{1,0:T(8,128)(2,1)} %key_hbm.1, bf16[2048,512]{1,0:T(8,128)(2,1)} %value_hbm.1, ...), custom_call_target="tpu_custom_call" | custom-call | tf_op jit(solution)/shard_map/pallas_call | solution.py:352
  39.4 4.7 %shard_map.195 = (bf16[48,2048]{1,0:T(8,128)(2,1)}, f32[48,8,64,64]{3,2,1,0:T(8,128)}) custom-call(bf16[48,2048]{1,0:T(8,128)(2,1)S(1)} %get-tuple-element.4.output, f32[48,8,64,64]{3,2,1,0:T(8,128)S(1)} %get-tuple-element.5.new_state), custom_call_target="tpu_custom_call" | custom-call | tf_op jit(solution)/shard_map/pallas_call | solution.py:379
